TPU v7x, 32 devices: a whole 2x2x4 slice. The times are simulated.
32 devices in a mesh: grp: 2 (over y), sp: 4 (over z), tp: 4 (over x, core).
Axes of the slice: x: 2, y: 2, z: 4, core: 2. Of those that a mesh axis runs over, the one named last changes fastest.
Arguments:
- queries: bfloat16 [2048, 512], P(('grp', 'sp'), 'tp'), parts along dimension 0, may hold values from -6 to 6
- key_rows: bfloat16 [2048, 512], P(('grp', 'sp'), 'tp'), parts along dimension 0, may hold values from -6 to 6
- value_rows: bfloat16 [2048, 1024], P(('grp', 'sp'), 'tp'), parts along dimension 0, may hold values from -6 to 6
- out_gate: bfloat16 [2048, 1024], P(('grp', 'sp'), 'tp'), parts along dimension 0, may hold values from -6 to 6
- log_decay: float32 [2, 2048, 512], P(None, ('grp', 'sp'), 'tp'), parts along dimension 1
- doc_ids: int32 [2048], P(('grp', 'sp')), parts along dimension 0, may hold values from 0 to 1, as said below
- head_gain: float32 [1024], P('tp'), may hold values from 0.1 to 1.9
- out_weight: bfloat16 [1024, 2048], P('tp'), may hold values from -0.375 to 0.375
- residual: bfloat16 [2048, 2048], P(('grp', 'sp'), 'tp'), parts along dimension 0
- norm_gain: float32 [2, 2048], replicated, may hold values from 0.1 to 1.9
- norm_bias: float32 [2, 2048], replicated, may hold values from -3 to 3
- gate_weight: bfloat16 [2048, 3072], P('sp', 'tp'), may hold values from -0.125 to 0.125
- up_weight: bfloat16 [2048, 3072], P('sp', 'tp'), may hold values from -0.125 to 0.125
- down_weight: bfloat16 [3072, 2048], P('tp', 'sp'), may hold values from -0.109375 to 0.109375
Outputs:
- layer_out: bfloat16 [2048, 2048], P(('grp', 'sp'), 'tp'), parts along dimension 0
There are 2 independent parts, one for each index of `grp`. A program takes and returns all parts, laid end to end along the dimension named above; an argument that names none is the same for every part. Nothing has to cross between parts.
Inputs may be any that keep to these rules, and one draw needn't show every extreme that they name: `doc_ids`: document numbers start at 0 and never fall; they rise by one at each of 1 positions, the k-th rise lying within half of 256 positions of k times 1024 divided by 2.
All inputs are finite; a program needn't handle non-finite values.
Results may differ from a plain program's by a relative error of at most 0.009.
Values may be sent and summed in bfloat16 or wider, within the bound.
A program may use at most 128 MiB of HBM per device.

v0:
```python
import jax
import jax.numpy as jnp
from jax import lax
from jax.sharding import PartitionSpec as P

DK = 32
DV = 64
BLOCK = 64
EPS = 1e-06
HIGH = lax.Precision.HIGHEST


def entering(x, axis, combine, identity, reverse):
    peers, position = (lax.axis_size(axis), lax.axis_index(axis))
    everything = jax.tree.map(
        lambda part, kind: lax.all_gather(part.astype(kind), axis),
        x,
        jax.tree.map(lambda a: jnp.bfloat16 if a.dtype == jnp.float32 else a.dtype, x),
    )
    start = jax.tree.map(
        lambda part, zero: jnp.broadcast_to(jnp.asarray(zero, part.dtype), part.shape), x, identity
    )

    def hop(k, before):
        at = peers - 1 - k if reverse else k
        reached = at > position if reverse else at < position
        new = combine(
            before, jax.tree.map(lambda part, own: part[at].astype(own.dtype), everything, x)
        )
        return jax.tree.map(lambda a, b: jnp.where(reached, a, b), new, before)

    return lax.fori_loop(0, peers, hop, start)


def run_blocks(query, key_part, value_part, decay, docs):
    length = query.shape[0]
    count = length // BLOCK
    head_count = query.shape[1]
    lower = jnp.arange(BLOCK)[:, None] >= jnp.arange(BLOCK)[None, :]

    def blocked(array):
        return array.reshape((count, BLOCK) + array.shape[1:])

    def advance(carried, inputs):
        state, state_doc = carried
        query_block, key_block, value_block, decay_block, doc_block = inputs
        running = jnp.cumsum(decay_block, axis=0)
        allowed = lower & (doc_block[:, None] == doc_block[None, :])
        relative = jnp.exp(
            jnp.where(allowed[:, :, None, None], running[:, None] - running[None, :], -jnp.inf)
        )
        scores = jnp.einsum("ihd,jhd,ijhd->hij", query_block, key_block, relative, precision=HIGH)
        within = jnp.einsum("hij,jhe->ihe", scores, value_block, precision=HIGH)
        linked = (doc_block == state_doc).astype(jnp.float32)
        carried_part = (
            jnp.einsum("ihd,hde->ihe", query_block * jnp.exp(running), state, precision=HIGH)
            * linked[:, None, None]
        )
        closing = doc_block[-1]
        ending = (doc_block == closing).astype(jnp.float32)
        tail_decay = jnp.exp(running[-1][None] - running) * ending[:, None, None]
        kept = (state_doc == closing).astype(jnp.float32)
        state = kept * jnp.exp(running[-1])[:, :, None] * state + jnp.einsum(
            "jhd,jhe->hde", key_block * tail_decay, value_block, precision=HIGH
        )
        return ((state, closing), within + carried_part)

    start = (
        jnp.zeros((head_count, query.shape[2], value_part.shape[2]), jnp.float32),
        jnp.array(-1, jnp.int32),
    )
    (state, closing), outputs = lax.scan(
        advance,
        start,
        tuple((blocked(array) for array in (query, key_part, value_part, decay, docs))),
    )
    return (outputs.reshape(length, head_count, value_part.shape[2]), state, closing)


def chain(earlier, later):
    early_state, early_pass, early_entry, early_leave = earlier
    late_state, late_pass, late_entry, late_leave = later
    joined = (late_entry == early_leave) | (early_leave < 0.0) | (late_entry < 0.0)
    keep = jnp.where(joined, jnp.float32(1.0), jnp.float32(0.0))
    state = late_state + keep * late_pass[:, :, None] * early_state
    passing = keep * early_pass * late_pass
    entry = jnp.where(early_entry < 0.0, late_entry, early_entry)
    leaving = jnp.where(late_leave < 0.0, early_leave, late_leave)
    return (state, passing, entry, leaving)


def one_way(query, key_part, value_part, decay, docs, backward):
    local_out, state, closing = run_blocks(query, key_part, value_part, decay, docs)
    passing = jnp.exp(jnp.sum(decay, axis=0)) * (docs[0] == closing).astype(jnp.float32)
    piece = (state, passing, docs[0].astype(jnp.float32), closing.astype(jnp.float32))
    identity = (jnp.zeros_like(state), jnp.ones_like(passing), jnp.float32(-1.0), jnp.float32(-1.0))
    if backward:
        carried = entering(piece, "sp", chain, identity, True)
    else:
        carried = entering(piece, "sp", chain, identity, False)
    incoming, _, _, leaving = carried
    linked = (docs.astype(jnp.float32) == leaving).astype(jnp.float32)
    reach = query * jnp.exp(jnp.cumsum(decay, axis=0))
    return (
        local_out
        + jnp.einsum("ihd,hde->ihe", reach, incoming, precision=HIGH) * linked[:, None, None]
    )


def apply_norm(stream, moments, full_width, gain, bias):
    middle = moments[0][:, None] / full_width
    spread = moments[1][:, None] / full_width - middle * middle
    return (stream - middle) * lax.rsqrt(spread + EPS) * gain + bias


def on_device(
    queries,
    key_rows,
    value_rows,
    out_gate,
    log_decay,
    doc_ids,
    head_gain,
    out_weight,
    residual,
    norm_gain,
    norm_bias,
    gate_weight,
    up_weight,
    down_weight,
):
    collected = None
    length = queries.shape[0]
    head_count = queries.shape[1] // DK
    query = queries.astype(jnp.float32).reshape(length, head_count, DK) * DK ** (-0.5)
    key_part = key_rows.astype(jnp.float32).reshape(length, head_count, DK)
    value_part = value_rows.astype(jnp.float32).reshape(length, head_count, DV)
    forward_decay = log_decay[0].reshape(length, head_count, DK)
    backward_decay = log_decay[1].reshape(length, head_count, DK)
    forward_out = one_way(query, key_part, value_part, forward_decay, doc_ids, False)
    backward_out = one_way(
        query[::-1], key_part[::-1], value_part[::-1], backward_decay[::-1], doc_ids[::-1], True
    )[::-1]
    attended = forward_out + backward_out
    normed = attended * lax.rsqrt(jnp.mean(attended * attended, axis=-1, keepdims=True) + EPS)
    mixed = (
        normed.reshape(length, -1) * head_gain * jax.nn.silu(out_gate.astype(jnp.float32))
    ).astype(jnp.bfloat16)
    partial_value = jnp.dot(mixed, out_weight, preferred_element_type=jnp.float32)
    collected = (
        lax.all_gather(gate_weight, "sp", axis=0, tiled=True),
        lax.all_gather(up_weight, "sp", axis=0, tiled=True),
        lax.all_gather(down_weight, "sp", axis=1, tiled=True),
    )
    gate_full, up_full, down_full = collected
    own_width = residual.shape[1]
    full_width = own_width * lax.axis_size("tp")
    offset = lax.axis_index("tp") * own_width
    branch = lax.psum_scatter(
        partial_value.astype(jnp.bfloat16), "tp", scatter_dimension=1, tiled=True
    ).astype(jnp.float32)
    stream = residual.astype(jnp.float32) + branch
    moments = lax.psum((jnp.sum(stream, axis=1), jnp.sum(stream * stream, axis=1)), "tp")
    settled = apply_norm(
        stream,
        moments,
        full_width,
        lax.dynamic_slice_in_dim(norm_gain[0], offset, own_width, 0),
        lax.dynamic_slice_in_dim(norm_bias[0], offset, own_width, 0),
    )
    features = settled.astype(jnp.bfloat16)
    piece = lax.all_gather(features, "tp", axis=1, tiled=True)
    gate = jnp.dot(piece, gate_full, preferred_element_type=jnp.float32)
    up_part = jnp.dot(piece, up_full, preferred_element_type=jnp.float32)
    inner = (jax.nn.silu(gate) * up_part).astype(jnp.bfloat16)
    down = lax.psum_scatter(
        jnp.dot(inner, down_full, preferred_element_type=jnp.float32).astype(jnp.bfloat16),
        "tp",
        scatter_dimension=1,
        tiled=True,
    ).astype(jnp.float32)
    final = settled + 0.5 * down
    closing_moments = lax.psum((jnp.sum(final, axis=1), jnp.sum(final * final, axis=1)), "tp")
    result = apply_norm(
        final,
        closing_moments,
        full_width,
        lax.dynamic_slice_in_dim(norm_gain[1], offset, own_width, 0),
        lax.dynamic_slice_in_dim(norm_bias[1], offset, own_width, 0),
    )
    return result.astype(jnp.bfloat16)


def solution(mesh):
    in_specs = (
        P(("grp", "sp"), "tp"),
        P(("grp", "sp"), "tp"),
        P(("grp", "sp"), "tp"),
        P(("grp", "sp"), "tp"),
        P(None, ("grp", "sp"), "tp"),
        P(("grp", "sp")),
        P("tp"),
        P("tp", None),
        P(("grp", "sp"), "tp"),
        P(),
        P(),
        P("sp", "tp"),
        P("sp", "tp"),
        P("tp", "sp"),
    )
    out_specs = P(("grp", "sp"), "tp")
    return jax.shard_map(
        on_device, mesh=mesh, in_specs=in_specs, out_specs=out_specs, check_vma=False
    )
```

profile of v0, /device:TPU:0, one launch (start us, length us, event | category | flops | bytes accessed | tf_op | source)
XLA Modules:
  0.0 599.7 jit_solution(14972712356723388708)
XLA Ops:
  20.4 91.4 %while.66 = (s32[]{:T(128)}, f32[4,32,64]{2,1,0:T(8,128)S(1)}, s32[]{:T(128)}, f32[4,64,4,64]{1,0,3,2:T(4,128)}, s32[4,64]{1,0:T(4,128)S(1)}, /*index=5*/f32[4,6...) while((s32[]{:T(128)}, f32[4,32,64]{2,1,0:T(8,128)S(1)}, ...), condition=%wide.region_10.11_spmd.clone, body=%wide.region_8.10_spmd.clone.sunk | while | flops 28397956 | bytes 10073782 | solution.py:72
  21.6 3.2 exponential_bitcast_fusion.11
  24.7 5.8 copy.268
  37.0 4.5 dynamic_update_slice.12
  44.4 3.2 exponential_bitcast_fusion.11
  47.6 5.8 copy.268
  59.8 4.5 dynamic_update_slice.12
  67.3 3.2 exponential_bitcast_fusion.11
  70.5 5.8 copy.268
  82.7 4.5 dynamic_update_slice.12
  90.2 3.2 exponential_bitcast_fusion.11
  93.3 5.8 copy.268
  105.6 4.5 dynamic_update_slice.12
  117.5 88.7 %while.64 = (s32[]{:T(128)}, f32[4,32,64]{2,1,0:T(8,128)S(1)}, s32[]{:T(128)}, f32[4,64,4,64]{1,0,3,2:T(4,128)}, s32[4,64]{1,0:T(4,128)S(1)}, /*index=5*/f32[4,6...) while((s32[]{:T(128)}, f32[4,32,64]{2,1,0:T(8,128)S(1)}, ...), condition=%wide.region_2.3_spmd.clone, body=%wide.region_0.2_spmd.clone.sunk | while | flops 28397956 | bytes 10237110 | solution.py:72
  121.2 3.2 exponential_bitcast_fusion.10
  124.3 5.8 copy.262
  130.3 2.9 fusion.122
  133.6 4.5 dynamic_update_slice.11
  143.4 3.2 exponential_bitcast_fusion.10
  146.5 5.8 copy.262
  152.5 2.9 fusion.122
  155.8 4.5 dynamic_update_slice.11
  165.5 3.2 exponential_bitcast_fusion.10
  168.7 5.8 copy.262
  174.7 2.9 fusion.122
  178.0 4.5 dynamic_update_slice.11
  187.7 3.2 exponential_bitcast_fusion.10
  190.9 5.8 copy.262
  196.9 2.9 fusion.122
  200.2 4.5 dynamic_update_slice.11
  208.7 12.7 %all-gather.3 = bf16[4,4,32]{2,1,0:T(4,128)(2,1)S(1)} all-gather(bf16[1,4,32]{2,1,0:T(4,128)(2,1)S(1)} %fusion.57), channel_id=4, replica_groups=mesh['grp'=2,'sp'=4,'tp'=4] {'sp'}, dimensions={0}, use_global_device_ids=true | all-gather | bytes 1280 | tf_op jit(solution)/shard_map/all_gather | solution.py:16
  221.4 13.4 %all-gather.1 = bf16[16,32,64]{2,1,0:T(8,128)(2,1)S(1)} all-gather(bf16[4,32,64]{2,1,0:T(8,128)(2,1)S(1)} %convert_element_type.257), channel_id=3, replica_groups=mesh['grp'=2,'sp'=4,'tp'=4] {'sp'}, dimensions={0}, use_global_device_ids=true | all-gather | bytes 81920 | tf_op jit(solution)/shard_map/all_gather | solution.py:16
  238.4 8.5 %all-reduce.6 = (bf16[4]{0:T(256)(128)(2,1)S(1)}, bf16[4]{0:T(256)(128)(2,1)S(1)}, bf16[4]{0:T(256)(128)(2,1)S(1)}, bf16[4]{0:T(256)(128)(2,1)S(1)}) all-reduce(bf16[4]{0:T(256)(128)(2,1)S(1)} %dynamic-update-slice.2, bf16[4]{0:T(256)(128)(2,1)S(1)} %dynamic-update-slice.3, ...), channel_id=1, replica_groups=mesh['grp'=2,'sp'=4,'tp'=4] {'sp'}, use_global_device_ids=true, to_apply=%add.2 | all-reduce | flops 16 | bytes 64
  246.9 15.9 %while.67 = (s32[]{:T(128)}, f32[4,32,64]{2,1,0:T(8,128)S(1)}, f32[]{:T(128)}, s32[]{:T(128)}, bf16[4,4,32,64]{3,2,1,0:T(8,128)(2,1)S(1)}, /*index=5*/bf16[4]{0:...) while((s32[]{:T(128)}, f32[4,32,64]{2,1,0:T(8,128)S(1)}, ...), condition=%wide.region_13.14_spmd.clone, body=%wide.region_12.13_spmd.clone.sunk | while | flops 41233 | bytes 83500 | solution.py:32
  263.2 4.3 reduce-window.16
  269.5 9.6 %all_gather.60 = bf16[4,4,32]{2,1,0:T(4,128)(2,1)S(1)} all-gather(bf16[1,4,32]{2,1,0:T(4,128)(2,1)S(1)} %convert_element_type.252), channel_id=1, replica_groups=mesh['grp'=2,'sp'=4,'tp'=4] {'sp'}, dimensions={0}, use_global_device_ids=true | all-gather | bytes 1280 | tf_op jit(solution)/shard_map/all_gather | solution.py:16
  279.1 13.4 %all-gather = bf16[16,32,64]{2,1,0:T(8,128)(2,1)S(1)} all-gather(bf16[4,32,64]{2,1,0:T(8,128)(2,1)S(1)} %convert_element_type.247), channel_id=2, replica_groups=mesh['grp'=2,'sp'=4,'tp'=4] {'sp'}, dimensions={0}, use_global_device_ids=true | all-gather | bytes 81920 | tf_op jit(solution)/shard_map/all_gather | solution.py:16
  292.5 15.8 %while.65 = (s32[]{:T(128)}, f32[4,32,64]{2,1,0:T(8,128)S(1)}, f32[]{:T(128)}, s32[]{:T(128)}, bf16[4,4,32,64]{3,2,1,0:T(8,128)(2,1)S(1)}, /*index=5*/bf16[4]{0:...) while((s32[]{:T(128)}, f32[4,32,64]{2,1,0:T(8,128)S(1)}, ...), condition=%wide.region_5.6_spmd.clone, body=%wide.region_4.5_spmd.clone.sunk | while | flops 41229 | bytes 83438 | solution.py:32
  313.6 23.0 %reduce-scatter.3.cloned.1.call-done = bf16[256,512]{1,0:T(8,128)(2,1)} async-done(((bf16[256,2048]{1,0:T(8,128)(2,1)}), bf16[256,512]{1,0:T(8,128)(2,1)}) %reduce-scatter.3.cloned.1.call-update) | async-done | bytes 262160 | tf_op jit(solution)/shard_map/reduce_scatter | solution.py:159
  337.8 5.8 all-reduce.5
  347.4 15.5 %all-gather.9.cloned.1.call-done = bf16[256,2048]{1,0:T(8,128)(2,1)} async-done(((bf16[256,512]{1,0:T(8,128)(2,1)}), bf16[256,2048]{1,0:T(8,128)(2,1)}) %all-gather.9.cloned.1.call-update) | async-done | bytes 1048592 | tf_op jit(solution)/shard_map/all_gather | solution.py:172
  362.9 65.1 %all-gather.11.cloned.1.call-done = bf16[2048,768]{1,0:T(8,128)(2,1)} async-done(((bf16[512,768]{1,0:T(8,128)(2,1)}), bf16[2048,768]{1,0:T(8,128)(2,1)}) %all-gather.11.cloned.1.call-update) | async-done | bytes 3145744 | tf_op jit(solution)/shard_map/all_gather | solution.py:151
  428.0 4.1 fusion.68
  432.1 59.5 %all-gather.13.cloned.1.call-done = bf16[2048,768]{1,0:T(8,128)(2,1)} async-done(((bf16[512,768]{1,0:T(8,128)(2,1)}), bf16[2048,768]{1,0:T(8,128)(2,1)}) %all-gather.13.cloned.1.call-update) | async-done | bytes 3145744 | tf_op jit(solution)/shard_map/all_gather | solution.py:152
  491.5 63.5 %all-gather.15.cloned.1.call-done = bf16[768,2048]{1,0:T(8,128)(2,1)} async-done(((bf16[768,512]{1,0:T(8,128)(2,1)}), bf16[768,2048]{1,0:T(8,128)(2,1)}) %all-gather.15.cloned.1.call-update) | async-done | bytes 3145744 | tf_op jit(solution)/shard_map/all_gather | solution.py:153
  555.1 6.2 %convolution_convert_fusion.1 = bf16[256,2048]{1,0:T(8,128)(2,1)} fusion(bf16[768,2048]{1,0:T(8,128)(2,1)} %all-gather.15.cloned.1.call-done, bf16[256,2048]{1,0:T(8,128)(2,1)S(1)} %copy-done.14, bf16[2048,768]{1,0:T(8,128)(2,1)} %all-gather.13.cloned.1.call-done, f32[256,768]{1,0:T(8,128)} %fusion.68), kind=kOutput, calls=%fused_computation.68 | convolution fusion | flops 1612316672 | bytes 9175040 | tf_op jit(solution)/shard_map/dot_general | solution.py:177
  561.3 23.6 %reduce-scatter.5.cloned.1.call-done = bf16[256,512]{1,0:T(8,128)(2,1)} async-done(((bf16[256,2048]{1,0:T(8,128)(2,1)}), bf16[256,512]{1,0:T(8,128)(2,1)}) %reduce-scatter.5.cloned.1.call-update) | async-done | bytes 262160 | tf_op jit(solution)/shard_map/reduce_scatter | solution.py:176
  586.2 5.8 all-reduce.4
  (305 shorter events, 97.7 us)
Async XLA Ops:
  6.5 305.4 %copy-start = (bf16[256,2048]{1,0:T(8,128)(2,1)S(1)}, bf16[256,2048]{1,0:T(8,128)(2,1)}, u32[]{:S(2)}) copy-start(bf16[256,2048]{1,0:T(8,128)(2,1)} %param.29) | copy-start | bytes 3145732
  6.5 330.2 %reduce-scatter.3.cloned.1.call-start = ((), (), s32[]{:S(2)}) async-start(), calls=%async_computation.2 | async-start | bytes 1310720 | tf_op jit(solution)/shard_map/reduce_scatter | solution.py:159
  14.6 98.4 %copy-start.5 = (f32[256,4,32]{0,2,1:T(8,128)}, f32[256,4,32]{0,2,1:T(8,128)S(1)}, u32[]{:S(2)}) copy-start(f32[256,4,32]{0,2,1:T(8,128)S(1)} %rev.19) | copy-start | bytes 393220
  16.6 3.8 copy-start.9
  17.4 3.0 copy-start.8
  114.7 2.9 copy-start.6
  117.5 117.2 %copy-start.17 = (u32[32]{0:T(128)S(1)}, u32[32]{0:T(128)}, u32[]{:S(2)}) copy-start(u32[32]{0:T(128)} %constant.182) | copy-start | bytes 388
  117.5 145.3 %copy-start.3 = (f32[4,64,4,64]{1,0,3,2:T(4,128)S(1)}, f32[4,64,4,64]{1,0,3,2:T(4,128)}, u32[]{:S(2)}) copy-start(f32[4,64,4,64]{1,0,3,2:T(4,128)} %get-tuple-element.457) | copy-start | bytes 786436
  206.3 102.0 %copy-start.11 = (s32[256]{0:T(256)S(1)}, s32[256]{0:T(256)}, u32[]{:S(2)}) copy-start(s32[256]{0:T(256)} %param.27) | copy-start | bytes 3076
  206.3 102.0 %copy-start.4 = (f32[4,64,4,64]{1,0,3,2:T(4,128)S(1)}, f32[4,64,4,64]{1,0,3,2:T(4,128)}, u32[]{:S(2)}) copy-start(f32[4,64,4,64]{1,0,3,2:T(4,128)} %get-tuple-element.452) | copy-start | bytes 786436
  206.3 102.4 %copy-start.7 = (f32[1,256,128]{1,2,0:T(8,128)S(1)}, f32[1,256,128]{1,2,0:T(8,128)}, u32[]{:S(2)}) copy-start(f32[1,256,128]{1,2,0:T(8,128)} %copy-done.6) | copy-start | bytes 393220
  206.3 104.9 %copy-start.10 = (bf16[256,128]{0,1:T(8,128)(2,1)S(1)}, bf16[256,128]{0,1:T(8,128)(2,1)}, u32[]{:S(2)}) copy-start(bf16[256,128]{0,1:T(8,128)(2,1)} %copy-done.9) | copy-start | bytes 196612
  246.9 65.1 %copy-start.15 = (bf16[256,256]{1,0:T(8,128)(2,1)S(1)}, bf16[256,256]{1,0:T(8,128)(2,1)}, u32[]{:S(2)}) copy-start(bf16[256,256]{1,0:T(8,128)(2,1)} %param.25) | copy-start | bytes 393220
  246.9 65.1 %copy-start.16 = (f32[256]{0:T(256)S(1)}, f32[256]{0:T(256)}, u32[]{:S(2)}) copy-start(f32[256]{0:T(256)} %param.28) | copy-start | bytes 3076
  292.5 21.1 %copy-start.12 = (f32[2,2048]{1,0:T(2,128)S(1)}, f32[2,2048]{1,0:T(2,128)}, u32[]{:S(2)}) copy-start(f32[2,2048]{1,0:T(2,128)} %param.31) | copy-start | bytes 49156
  292.5 21.1 %copy-start.13 = (f32[2,2048]{1,0:T(2,128)S(1)}, f32[2,2048]{1,0:T(2,128)}, u32[]{:S(2)}) copy-start(f32[2,2048]{1,0:T(2,128)} %param.32) | copy-start | bytes 49156
  292.5 44.2 %copy-start.1 = (bf16[256,512]{1,0:T(8,128)(2,1)S(1)}, bf16[256,512]{1,0:T(8,128)(2,1)}, u32[]{:S(2)}) copy-start(bf16[256,512]{1,0:T(8,128)(2,1)} %param.30) | copy-start | bytes 786436
  313.5 49.4 %all-gather.9.cloned.1.call-start = ((), (), s32[]{:S(2)}) async-start(), calls=%async_computation.3 | async-start | bytes 1310720 | tf_op jit(solution)/shard_map/all_gather | solution.py:172
  345.5 82.5 %all-gather.11.cloned.1.call-start = ((), (), s32[]{:S(2)}) async-start(), calls=%async_computation.4 | async-start | bytes 3932160 | tf_op jit(solution)/shard_map/all_gather | solution.py:151
  346.2 145.3 %all-gather.13.cloned.1.call-start = ((), (), s32[]{:S(2)}) async-start(), calls=%async_computation.5 | async-start | bytes 3932160 | tf_op jit(solution)/shard_map/all_gather | solution.py:152
  346.8 208.3 %all-gather.15.cloned.1.call-start = ((), (), s32[]{:S(2)}) async-start(), calls=%async_computation.6 | async-start | bytes 3932160 | tf_op jit(solution)/shard_map/all_gather | solution.py:153
  347.4 237.5 %reduce-scatter.5.cloned.1.call-start = ((), (), s32[]{:S(2)}) async-start(), calls=%async_computation.7 | async-start | bytes 1310720 | tf_op jit(solution)/shard_map/reduce_scatter | solution.py:176
  362.9 192.1 %copy-start.14 = (bf16[256,2048]{1,0:T(8,128)(2,1)S(1)}, bf16[256,2048]{1,0:T(8,128)(2,1)}, u32[]{:S(2)}) copy-start(bf16[256,2048]{1,0:T(8,128)(2,1)} %all-gather.9.cloned.1.call-done) | copy-start | bytes 3145732
  432.1 152.8 %copy-start.2 = (bf16[256,512]{1,0:T(8,128)(2,1)S(1)}, bf16[256,512]{1,0:T(8,128)(2,1)}, u32[]{:S(2)}) copy-start(bf16[256,512]{1,0:T(8,128)(2,1)} %reduce-scatter.3.cloned.1.call-done) | copy-start | bytes 786436
Sparse Core Ops, SparseCore 0:
  313.6 23.0 reduce-scatter.2
  345.6 17.3 all-gather.8
  364.5 63.4 all-gather.10
  429.4 62.0 all-gather.12
  492.9 62.0 all-gather.14
  561.4 23.4 reduce-scatter.4
where the time goes:
time: 603 us; the launch traced here: 600 us
  waiting for transfers between devices  252 us (42%)
  local copies, waits for them, and re-layouts  132 us (22%)
  other arithmetic  75.6 us (13%)
  blocking collectives  69.1 us (11%)
  loops' own time  32.7 us (5%)
  matrix products  22 us (4%)
  between operations  16.4 us (3%)
    all_gather x1, waiting for transfers between devices, on_device(): lax.all_gather(gate_weight, 'sp', axis=0, tiled=True)  65.1 us
    all_gather x1, waiting for transfers between devices, on_device(): lax.all_gather(down_weight, 'sp', axis=1, tiled=True)  63.5 us
    all_gather x1, waiting for transfers between devices, on_device(): lax.all_gather(up_weight, 'sp', axis=0, tiled=True)  59.5 us
    all_gather x4, blocking collectives, entering(): lax.all_gather(part.astype(kind), axis)  49 us
    while x8, local copies, waits for them, and re-layouts  46.3 us
    dynamic_update_slice x8, local copies, waits for them, and re-layouts, run_blocks(): lax.scan(advance, start, tuple((blocked(array) for array in (query, key_p...  35.8 us
    while x8, other arithmetic  25.3 us
    reduce_scatter x1, waiting for transfers between devices, on_device(): lax.psum_scatter(jnp.dot(inner, down_full, preferred_element_type=jnp.flo...  23.6 us
  transfers between devices with their start and end apart: 6, of which 6 were waited for; matrix products, arithmetic and copies ran while one was open for 1% of the time, Pallas kernels for 0%

commit v1 on v0

--- a/solution.py
+++ b/solution.py
@@ -8,6 +8,11 @@
 BLOCK = 64
 EPS = 1e-06
 HIGH = lax.Precision.HIGHEST
+
+
+def all_parts(array, axis, along):
+    blocks = lax.all_gather(array, axis)
+    return jnp.concatenate(blocks, axis=along)
 
 
 def entering(x, axis, combine, identity, reverse):
@@ -150,7 +155,7 @@
     collected = (
         lax.all_gather(gate_weight, "sp", axis=0, tiled=True),
         lax.all_gather(up_weight, "sp", axis=0, tiled=True),
-        lax.all_gather(down_weight, "sp", axis=1, tiled=True),
+        all_parts(down_weight, "sp", 1),
     )
     gate_full, up_full, down_full = collected
     own_width = residual.shape[1]

time: 603 us -> 571 us (0.947)
  waiting for transfers between devices: 252 us -> 214 us
    all_gather x1, waiting for transfers between devices: 63.5 us -> 30 us  [all_parts(): blocks = lax.all_gather(array, axis)]
  transfers between devices with their start and end apart: 6 -> 6, of which waited for: 6 -> 6; matrix products, arithmetic and copies ran while one was open for 1% -> 2% of each run, Pallas kernels for 0% -> 0%
where the time goes in v1:
time: 571 us; the launch traced here: 568 us
  waiting for transfers between devices  214 us (37%)
  local copies, waits for them, and re-layouts  136 us (24%)
  other arithmetic  75.6 us (13%)
  blocking collectives  69.4 us (12%)
  loops' own time  32.7 us (6%)
  matrix products  22 us (4%)
  between operations  18.1 us (3%)
    all_gather x1, waiting for transfers between devices, on_device(): lax.all_gather(gate_weight, 'sp', axis=0, tiled=True)  64.8 us
    all_gather x1, waiting for transfers between devices, on_device(): lax.all_gather(up_weight, 'sp', axis=0, tiled=True)  59.5 us
    all_gather x4, blocking collectives, entering(): lax.all_gather(part.astype(kind), axis)  49 us
    while x8, local copies, waits for them, and re-layouts  46.3 us
    dynamic_update_slice x8, local copies, waits for them, and re-layouts, run_blocks(): lax.scan(advance, start, tuple((blocked(array) for array in (query, key_p...  35.8 us
    all_gather x1, waiting for transfers between devices, all_parts(): blocks = lax.all_gather(array, axis)  30 us
    while x8, other arithmetic  25.3 us
    reduce_scatter x1, waiting for transfers between devices, on_device(): lax.psum_scatter(jnp.dot(inner, down_full, preferred_element_type=jnp.flo...  23.6 us
  transfers between devices with their start and end apart: 6, of which 6 were waited for; matrix products, arithmetic and copies ran while one was open for 2% of the time, Pallas kernels for 0%

profile of v1, /device:TPU:0, one launch (start us, length us, event | category | flops | bytes accessed | tf_op | source)
XLA Modules:
  0.0 568.4 jit_solution(12712363311007943028)
XLA Ops:
  21.2 91.4 %while.66 = (s32[]{:T(128)}, f32[4,32,64]{2,1,0:T(8,128)S(1)}, s32[]{:T(128)}, f32[4,64,4,64]{1,0,3,2:T(4,128)}, s32[4,64]{1,0:T(4,128)S(1)}, /*index=5*/f32[4,6...) while((s32[]{:T(128)}, f32[4,32,64]{2,1,0:T(8,128)S(1)}, ...), condition=%wide.region_10.11_spmd.clone, body=%wide.region_8.10_spmd.clone.sunk | while | flops 28397956 | bytes 10073782 | solution.py:77
  22.4 3.2 exponential_bitcast_fusion.11
  25.6 5.8 %copy.305 = f32[4,64,64,32]{1,2,3,0:T(8,128)} copy(f32[4,64,64,32]{2,3,0,1:T(8,128)} %exponential_bitcast_fusion.11) | data formatting | bytes 4194304 | tf_op jit(solution)/shard_map/while
  37.8 4.5 dynamic_update_slice.12
  45.3 3.2 exponential_bitcast_fusion.11
  48.4 5.8 %copy.305 = f32[4,64,64,32]{1,2,3,0:T(8,128)} copy(f32[4,64,64,32]{2,3,0,1:T(8,128)} %exponential_bitcast_fusion.11) | data formatting | bytes 4194304 | tf_op jit(solution)/shard_map/while
  60.7 4.5 dynamic_update_slice.12
  68.1 3.2 exponential_bitcast_fusion.11
  71.3 5.8 %copy.305 = f32[4,64,64,32]{1,2,3,0:T(8,128)} copy(f32[4,64,64,32]{2,3,0,1:T(8,128)} %exponential_bitcast_fusion.11) | data formatting | bytes 4194304 | tf_op jit(solution)/shard_map/while
  83.5 4.5 dynamic_update_slice.12
  91.0 3.2 exponential_bitcast_fusion.11
  94.2 5.8 %copy.305 = f32[4,64,64,32]{1,2,3,0:T(8,128)} copy(f32[4,64,64,32]{2,3,0,1:T(8,128)} %exponential_bitcast_fusion.11) | data formatting | bytes 4194304 | tf_op jit(solution)/shard_map/while
  106.4 4.5 dynamic_update_slice.12
  118.4 88.7 %while.64 = (s32[]{:T(128)}, f32[4,32,64]{2,1,0:T(8,128)S(1)}, s32[]{:T(128)}, f32[4,64,4,64]{1,0,3,2:T(4,128)}, s32[4,64]{1,0:T(4,128)S(1)}, /*index=5*/f32[4,6...) while((s32[]{:T(128)}, f32[4,32,64]{2,1,0:T(8,128)S(1)}, ...), condition=%wide.region_2.3_spmd.clone, body=%wide.region_0.2_spmd.clone.sunk | while | flops 28397956 | bytes 10237110 | solution.py:77
  122.0 3.2 exponential_bitcast_fusion.10
  125.2 5.8 %copy.299 = f32[4,64,64,32]{1,2,3,0:T(8,128)} copy(f32[4,64,64,32]{2,3,0,1:T(8,128)} %exponential_bitcast_fusion.10) | data formatting | bytes 4194304 | tf_op jit(solution)/shard_map/while
  131.1 2.9 fusion.122
  134.4 4.5 dynamic_update_slice.11
  144.2 3.2 exponential_bitcast_fusion.10
  147.4 5.8 %copy.299 = f32[4,64,64,32]{1,2,3,0:T(8,128)} copy(f32[4,64,64,32]{2,3,0,1:T(8,128)} %exponential_bitcast_fusion.10) | data formatting | bytes 4194304 | tf_op jit(solution)/shard_map/while
  153.3 2.9 fusion.122
  156.6 4.5 dynamic_update_slice.11
  166.4 3.2 exponential_bitcast_fusion.10
  169.5 5.8 %copy.299 = f32[4,64,64,32]{1,2,3,0:T(8,128)} copy(f32[4,64,64,32]{2,3,0,1:T(8,128)} %exponential_bitcast_fusion.10) | data formatting | bytes 4194304 | tf_op jit(solution)/shard_map/while
  175.5 2.9 fusion.122
  178.8 4.5 dynamic_update_slice.11
  188.6 3.2 exponential_bitcast_fusion.10
  191.7 5.8 %copy.299 = f32[4,64,64,32]{1,2,3,0:T(8,128)} copy(f32[4,64,64,32]{2,3,0,1:T(8,128)} %exponential_bitcast_fusion.10) | data formatting | bytes 4194304 | tf_op jit(solution)/shard_map/while
  201.0 4.5 dynamic_update_slice.11
  209.5 12.7 %all-gather.4 = bf16[4,4,32]{2,1,0:T(4,128)(2,1)S(1)} all-gather(bf16[1,4,32]{2,1,0:T(4,128)(2,1)S(1)} %fusion.57), channel_id=4, replica_groups=mesh['grp'=2,'sp'=4,'tp'=4] {'sp'}, dimensions={0}, use_global_device_ids=true | all-gather | bytes 1280 | tf_op jit(solution)/shard_map/all_gather | solution.py:21
  222.2 13.4 %all-gather.1 = bf16[16,32,64]{2,1,0:T(8,128)(2,1)S(1)} all-gather(bf16[4,32,64]{2,1,0:T(8,128)(2,1)S(1)} %convert_element_type.257), channel_id=3, replica_groups=mesh['grp'=2,'sp'=4,'tp'=4] {'sp'}, dimensions={0}, use_global_device_ids=true | all-gather | bytes 81920 | tf_op jit(solution)/shard_map/all_gather | solution.py:21
  239.2 8.5 %all-reduce.6 = (bf16[4]{0:T(256)(128)(2,1)S(1)}, bf16[4]{0:T(256)(128)(2,1)S(1)}, bf16[4]{0:T(256)(128)(2,1)S(1)}, bf16[4]{0:T(256)(128)(2,1)S(1)}) all-reduce(bf16[4]{0:T(256)(128)(2,1)S(1)} %dynamic-update-slice.2, bf16[4]{0:T(256)(128)(2,1)S(1)} %dynamic-update-slice.3, ...), channel_id=1, replica_groups=mesh['grp'=2,'sp'=4,'tp'=4] {'sp'}, use_global_device_ids=true, to_apply=%add.2 | all-reduce | flops 16 | bytes 64
  247.7 15.9 %while.67 = (s32[]{:T(128)}, f32[4,32,64]{2,1,0:T(8,128)S(1)}, f32[]{:T(128)}, s32[]{:T(128)}, bf16[4,4,32,64]{3,2,1,0:T(8,128)(2,1)S(1)}, /*index=5*/bf16[4]{0:...) while((s32[]{:T(128)}, f32[4,32,64]{2,1,0:T(8,128)S(1)}, ...), condition=%wide.region_13.14_spmd.clone, body=%wide.region_12.13_spmd.clone.sunk | while | flops 41233 | bytes 83500 | solution.py:37
  264.0 4.3 reduce-window.16
  270.3 9.6 %all_gather.63 = bf16[4,4,32]{2,1,0:T(4,128)(2,1)S(1)} all-gather(bf16[1,4,32]{2,1,0:T(4,128)(2,1)S(1)} %convert_element_type.252), channel_id=1, replica_groups=mesh['grp'=2,'sp'=4,'tp'=4] {'sp'}, dimensions={0}, use_global_device_ids=true | all-gather | bytes 1280 | tf_op jit(solution)/shard_map/all_gather | solution.py:21
  279.9 13.4 %all-gather = bf16[16,32,64]{2,1,0:T(8,128)(2,1)S(1)} all-gather(bf16[4,32,64]{2,1,0:T(8,128)(2,1)S(1)} %convert_element_type.247), channel_id=2, replica_groups=mesh['grp'=2,'sp'=4,'tp'=4] {'sp'}, dimensions={0}, use_global_device_ids=true | all-gather | bytes 81920 | tf_op jit(solution)/shard_map/all_gather | solution.py:21
  293.3 15.8 %while.65 = (s32[]{:T(128)}, f32[4,32,64]{2,1,0:T(8,128)S(1)}, f32[]{:T(128)}, s32[]{:T(128)}, bf16[4,4,32,64]{3,2,1,0:T(8,128)(2,1)S(1)}, /*index=5*/bf16[4]{0:...) while((s32[]{:T(128)}, f32[4,32,64]{2,1,0:T(8,128)S(1)}, ...), condition=%wide.region_5.6_spmd.clone, body=%wide.region_4.5_spmd.clone.sunk | while | flops 41229 | bytes 83438 | solution.py:37
  315.1 22.5 %reduce-scatter.3.cloned.1.call-done = bf16[256,512]{1,0:T(8,128)(2,1)} async-done(((bf16[256,2048]{1,0:T(8,128)(2,1)}), bf16[256,512]{1,0:T(8,128)(2,1)}) %reduce-scatter.3.cloned.1.call-update) | async-done | bytes 262160 | tf_op jit(solution)/shard_map/reduce_scatter | solution.py:164
  338.7 6.1 %all-reduce.5 = (f32[256]{0:T(256)S(1)}, f32[256]{0:T(256)S(1)}) all-reduce(f32[256]{0:T(256)S(1)} %get-tuple-element.673, f32[256]{0:T(256)S(1)} %get-tuple-element.672), channel_id=1, replica_groups=mesh['grp'=2,'sp'=4,'tp'=4] {'tp'}, use_global_device_ids=true, to_apply=%region_21.22 | all-reduce | flops 512 | bytes 4096 | tf_op jit(solution)/shard_map/psum | solution.py:168
  348.0 30.0 %all-gather.16.cloned.1.call-done = bf16[3072,512]{1,0:T(8,128)(2,1)} async-done(((bf16[768,512]{1,0:T(8,128)(2,1)}), bf16[3072,512]{1,0:T(8,128)(2,1)}) %all-gather.16.cloned.1.call-update) | async-done | bytes 3145744 | tf_op jit(solution)/shard_map/all_gather | solution.py:14
  378.0 4.7 copy.204
  382.7 12.0 %all-gather.10.cloned.1.call-done = bf16[256,2048]{1,0:T(8,128)(2,1)} async-done(((bf16[256,512]{1,0:T(8,128)(2,1)}), bf16[256,2048]{1,0:T(8,128)(2,1)}) %all-gather.10.cloned.1.call-update) | async-done | bytes 1048592 | tf_op jit(solution)/shard_map/all_gather | solution.py:177
  394.7 64.8 %all-gather.12.cloned.1.call-done = bf16[2048,768]{1,0:T(8,128)(2,1)} async-done(((bf16[512,768]{1,0:T(8,128)(2,1)}), bf16[2048,768]{1,0:T(8,128)(2,1)}) %all-gather.12.cloned.1.call-update) | async-done | bytes 3145744 | tf_op jit(solution)/shard_map/all_gather | solution.py:156
  459.4 4.1 fusion.68
  463.5 59.5 %all-gather.14.cloned.1.call-done = bf16[2048,768]{1,0:T(8,128)(2,1)} async-done(((bf16[512,768]{1,0:T(8,128)(2,1)}), bf16[2048,768]{1,0:T(8,128)(2,1)}) %all-gather.14.cloned.1.call-update) | async-done | bytes 3145744 | tf_op jit(solution)/shard_map/all_gather | solution.py:157
  523.0 6.3 %convolution_convert_fusion.1 = bf16[256,2048]{1,0:T(8,128)(2,1)} fusion(bf16[768,2048]{0,1:T(8,128)(2,1)} %bitcast.312, bf16[256,2048]{1,0:T(8,128)(2,1)S(1)} %copy-done.14, bf16[2048,768]{1,0:T(8,128)(2,1)} %all-gather.14.cloned.1.call-done, f32[256,768]{1,0:T(8,128)} %fusion.68), kind=kOutput, calls=%fused_computation.68 | convolution fusion | flops 1612316672 | bytes 9175040 | tf_op jit(solution)/shard_map/dot_general | solution.py:182
  529.3 23.6 %reduce-scatter.5.cloned.1.call-done = bf16[256,512]{1,0:T(8,128)(2,1)} async-done(((bf16[256,2048]{1,0:T(8,128)(2,1)}), bf16[256,512]{1,0:T(8,128)(2,1)}) %reduce-scatter.5.cloned.1.call-update) | async-done | bytes 262160 | tf_op jit(solution)/shard_map/reduce_scatter | solution.py:181
  554.2 5.8 %all-reduce.4 = (f32[256]{0:T(256)S(1)}, f32[256]{0:T(256)S(1)}) all-reduce(f32[256]{0:T(256)S(1)} %get-tuple-element.671, f32[256]{0:T(256)S(1)} %get-tuple-element.670), channel_id=1, replica_groups=mesh['grp'=2,'sp'=4,'tp'=4] {'tp'}, use_global_device_ids=true, to_apply=%region_26.27 | all-reduce | flops 512 | bytes 4096 | tf_op jit(solution)/shard_map/psum | solution.py:188
  (306 shorter events, 100.6 us)
Async XLA Ops:
  7.4 305.5 %copy-start = (bf16[256,2048]{1,0:T(8,128)(2,1)S(1)}, bf16[256,2048]{1,0:T(8,128)(2,1)}, u32[]{:S(2)}) copy-start(bf16[256,2048]{1,0:T(8,128)(2,1)} %param.29) | copy-start | bytes 3145732
  7.4 330.2 %reduce-scatter.3.cloned.1.call-start = ((), (), s32[]{:S(2)}) async-start(), calls=%async_computation.2 | async-start | bytes 1310720 | tf_op jit(solution)/shard_map/reduce_scatter | solution.py:164
  15.4 98.4 %copy-start.5 = (f32[256,4,32]{0,2,1:T(8,128)}, f32[256,4,32]{0,2,1:T(8,128)S(1)}, u32[]{:S(2)}) copy-start(f32[256,4,32]{0,2,1:T(8,128)S(1)} %rev.19) | copy-start | bytes 393220
  17.4 3.8 copy-start.9
  18.2 3.0 copy-start.8
  115.5 2.9 copy-start.6
  118.4 117.2 %copy-start.17 = (u32[32]{0:T(128)S(1)}, u32[32]{0:T(128)}, u32[]{:S(2)}) copy-start(u32[32]{0:T(128)} %constant.182) | copy-start | bytes 388
  118.4 145.3 %copy-start.3 = (f32[4,64,4,64]{1,0,3,2:T(4,128)S(1)}, f32[4,64,4,64]{1,0,3,2:T(4,128)}, u32[]{:S(2)}) copy-start(f32[4,64,4,64]{1,0,3,2:T(4,128)} %get-tuple-element.457) | copy-start | bytes 786436
  207.1 102.0 %copy-start.11 = (s32[256]{0:T(256)S(1)}, s32[256]{0:T(256)}, u32[]{:S(2)}) copy-start(s32[256]{0:T(256)} %param.27) | copy-start | bytes 3076
  207.1 102.1 %copy-start.4 = (f32[4,64,4,64]{1,0,3,2:T(4,128)S(1)}, f32[4,64,4,64]{1,0,3,2:T(4,128)}, u32[]{:S(2)}) copy-start(f32[4,64,4,64]{1,0,3,2:T(4,128)} %get-tuple-element.452) | copy-start | bytes 786436
  207.1 102.4 %copy-start.7 = (f32[1,256,128]{1,2,0:T(8,128)S(1)}, f32[1,256,128]{1,2,0:T(8,128)}, u32[]{:S(2)}) copy-start(f32[1,256,128]{1,2,0:T(8,128)} %copy-done.6) | copy-start | bytes 393220
  207.1 105.0 %copy-start.10 = (bf16[256,128]{0,1:T(8,128)(2,1)S(1)}, bf16[256,128]{0,1:T(8,128)(2,1)}, u32[]{:S(2)}) copy-start(bf16[256,128]{0,1:T(8,128)(2,1)} %copy-done.9) | copy-start | bytes 196612
  247.7 65.1 %copy-start.15 = (bf16[256,256]{1,0:T(8,128)(2,1)S(1)}, bf16[256,256]{1,0:T(8,128)(2,1)}, u32[]{:S(2)}) copy-start(bf16[256,256]{1,0:T(8,128)(2,1)} %param.25) | copy-start | bytes 393220
  247.7 65.1 %copy-start.16 = (f32[256]{0:T(256)S(1)}, f32[256]{0:T(256)}, u32[]{:S(2)}) copy-start(f32[256]{0:T(256)} %param.28) | copy-start | bytes 3076
  309.1 5.9 %copy-start.12 = (f32[2,2048]{1,0:T(2,128)S(1)}, f32[2,2048]{1,0:T(2,128)}, u32[]{:S(2)}) copy-start(f32[2,2048]{1,0:T(2,128)} %param.31) | copy-start | bytes 49156
  309.1 5.9 %copy-start.13 = (f32[2,2048]{1,0:T(2,128)S(1)}, f32[2,2048]{1,0:T(2,128)}, u32[]{:S(2)}) copy-start(f32[2,2048]{1,0:T(2,128)} %param.32) | copy-start | bytes 49156
  309.1 28.4 %copy-start.1 = (bf16[256,512]{1,0:T(8,128)(2,1)S(1)}, bf16[256,512]{1,0:T(8,128)(2,1)}, u32[]{:S(2)}) copy-start(bf16[256,512]{1,0:T(8,128)(2,1)} %param.30) | copy-start | bytes 786436
  314.4 63.6 %all-gather.16.cloned.1.call-start = ((), (), s32[]{:S(2)}) async-start(), calls=%async_computation.7 | async-start | bytes 3932160 | tf_op jit(solution)/shard_map/all_gather | solution.py:14
  314.9 79.7 %all-gather.10.cloned.1.call-start = ((), (), s32[]{:S(2)}) async-start(), calls=%async_computation.3 | async-start | bytes 1310720 | tf_op jit(solution)/shard_map/all_gather | solution.py:177
  346.6 112.8 %all-gather.12.cloned.1.call-start = ((), (), s32[]{:S(2)}) async-start(), calls=%async_computation.4 | async-start | bytes 3932160 | tf_op jit(solution)/shard_map/all_gather | solution.py:156
  347.2 175.8 %all-gather.14.cloned.1.call-start = ((), (), s32[]{:S(2)}) async-start(), calls=%async_computation.5 | async-start | bytes 3932160 | tf_op jit(solution)/shard_map/all_gather | solution.py:157
  347.9 204.9 %reduce-scatter.5.cloned.1.call-start = ((), (), s32[]{:S(2)}) async-start(), calls=%async_computation.6 | async-start | bytes 1310720 | tf_op jit(solution)/shard_map/reduce_scatter | solution.py:181
  394.7 128.4 %copy-start.14 = (bf16[256,2048]{1,0:T(8,128)(2,1)S(1)}, bf16[256,2048]{1,0:T(8,128)(2,1)}, u32[]{:S(2)}) copy-start(bf16[256,2048]{1,0:T(8,128)(2,1)} %all-gather.10.cloned.1.call-done) | copy-start | bytes 3145732
  523.0 29.9 %copy-start.2 = (bf16[256,512]{1,0:T(8,128)(2,1)S(1)}, bf16[256,512]{1,0:T(8,128)(2,1)}, u32[]{:S(2)}) copy-start(bf16[256,512]{1,0:T(8,128)(2,1)} %reduce-scatter.3.cloned.1.call-done) | copy-start | bytes 786436
Sparse Core Ops, SparseCore 0:
  314.5 23.0 reduce-scatter.2
  529.4 23.4 reduce-scatter.4
Sparse Core Ops, SparseCore 1:
  316.4 61.5 all-gather.15
  379.4 15.2 all-gather.9
  396.1 63.3 all-gather.11
  461.0 61.9 all-gather.13
